TPU v7x, 32 devices: a whole 2x2x4 slice. The times are simulated.
32 devices in a mesh: fs: 8 (over z, y), tp: 4 (over x, core).
Axes of the slice: x: 2, y: 2, z: 4, core: 2. Of those that a mesh axis runs over, the one named last changes fastest.
Arguments:
- tokens: bfloat16 [8192, 2048], P('fs', 'tp'), may hold values from -6 to 6
- mix_gain: float32 [2048], replicated, may hold values from 0.1 to 1.9
- in_weight: float32 [2048, 1024], P('fs', 'tp'), may hold values from -0.125 to 0.125
- in_scale: float32 [1024], P('tp'), may hold values from 0.4 to 2.5
- out_weight: float32 [1024, 2048], P('tp', 'fs'), may hold values from -0.1875 to 0.1875
- out_scale: float32 [2048], P('fs'), may hold values from 0.4 to 2.5
- ffn_gain: float32 [2048], replicated, may hold values from 0.1 to 1.9
- gate_weight: float32 [2048, 6144], P('fs', 'tp'), may hold values from -0.125 to 0.125
- gate_scale: float32 [6144], P('tp'), may hold values from 0.4 to 2.5
- up_weight: float32 [2048, 6144], P('fs', 'tp'), may hold values from -0.125 to 0.125
- up_scale: float32 [6144], P('tp'), may hold values from 0.4 to 2.5
- down_weight: float32 [6144, 2048], P('tp', 'fs'), may hold values from -0.078125 to 0.078125
- down_scale: float32 [2048], P('fs'), may hold values from 0.4 to 2.5
Outputs:
- layer_out: bfloat16 [8192, 2048], P('fs', 'tp')
All inputs are finite; a program needn't handle non-finite values.
Results may differ from a plain program's by a relative error of at most 0.023.
Values may be sent and summed in bfloat16 or wider, within the bound.
A program may use at most 128 MiB of HBM per device.

v0:
```python
import jax
import jax.numpy as jnp
from jax import lax
from jax.sharding import PartitionSpec as P

D = 2048
GROUPS = 4
GRID_W = 64
GC = 256
WINDOWS = (2, 4, 8, 16)
EPSILON = 1e-06


def box_matrix(length, window):
    position = jnp.arange(length, dtype=jnp.int32)
    lower_end = jnp.clip(position - window // 2, 0, length)
    upper_end = jnp.clip(position + (window - window // 2), 0, length)
    inside = (position[None, :] >= lower_end[:, None]) & (position[None, :] < upper_end[:, None])
    return inside.astype(jnp.float32) / (upper_end - lower_end).astype(jnp.float32)[:, None]


def pooled_differences(channels, channel_offset):
    tokens_here, extent = channels.shape
    lattice = channels.reshape(tokens_here // GRID_W, GRID_W, extent)
    group_of = (channel_offset + jnp.arange(extent, dtype=jnp.int32)) // GC
    result = jnp.zeros_like(lattice)
    for group in range(GROUPS):
        window = WINDOWS[group]
        across = jnp.einsum(
            "jk,akc->ajc", box_matrix(GRID_W, window), lattice, precision=lax.Precision.HIGHEST
        )
        smoothed = jnp.einsum(
            "ab,bjc->ajc",
            box_matrix(lattice.shape[0], window),
            across,
            precision=lax.Precision.HIGHEST,
        )
        result = jnp.where((group_of == group)[None, None, :], smoothed, result)
    return (result - lattice).reshape(tokens_here, extent).astype(jnp.bfloat16)


def fold_rows(features, gain, weights):
    widened = lax.all_gather(features, "tp", axis=1, tiled=True).astype(jnp.float32)
    squares = jnp.sum(widened * widened, axis=1)
    scaled = (widened * gain).astype(jnp.bfloat16)
    totals = tuple(
        (jnp.dot(scaled, weight, preferred_element_type=jnp.float32) for weight in weights)
    )
    totals, squares = (totals, squares)
    inverse_rms = lax.rsqrt(squares / D + EPSILON)[:, None]
    return tuple((total * inverse_rms for total in totals))


def column_product(hidden, weight_columns, scales):
    partial_value = (
        jnp.dot(
            hidden,
            lax.all_gather(weight_columns, "fs", axis=1, tiled=True),
            preferred_element_type=jnp.float32,
        )
        * scales
    )
    return lax.psum_scatter(
        partial_value.astype(jnp.bfloat16), "tp", scatter_dimension=1, tiled=True
    ).astype(jnp.float32)


def local(
    tokens,
    mix_gain,
    in_weight,
    in_scale,
    out_weight,
    out_scale,
    ffn_gain,
    gate_weight,
    gate_scale,
    up_weight,
    up_scale,
    down_weight,
    down_scale,
):
    out_scales, down_scales = (
        lax.all_gather(out_scale, "fs", axis=0, tiled=True),
        lax.all_gather(down_scale, "fs", axis=0, tiled=True),
    )
    in_full, gate_full, up_full = (
        lax.all_gather(in_weight.astype(jnp.bfloat16), "fs", axis=0, tiled=True),
        lax.all_gather(gate_weight.astype(jnp.bfloat16), "fs", axis=0, tiled=True),
        lax.all_gather(up_weight.astype(jnp.bfloat16), "fs", axis=0, tiled=True),
    )
    (channels,) = fold_rows(tokens, mix_gain, (in_full,))
    channels = channels * in_scale
    pooled = pooled_differences(channels, lax.axis_index("tp") * channels.shape[1])
    mixed = column_product(pooled, out_weight.astype(jnp.bfloat16), out_scales)
    residual = (tokens.astype(jnp.float32) + mixed).astype(jnp.bfloat16)
    gate_value, up_value = fold_rows(residual, ffn_gain, (gate_full, up_full))
    gate_value = gate_value * gate_scale
    up_value = up_value * up_scale
    hidden = (jax.nn.silu(gate_value) * up_value).astype(jnp.bfloat16)
    channel_out = column_product(hidden, down_weight.astype(jnp.bfloat16), down_scales)
    return (residual.astype(jnp.float32) + channel_out).astype(jnp.bfloat16)


def solution(mesh):
    return jax.shard_map(
        local,
        mesh=mesh,
        in_specs=(
            P("fs", "tp"),
            P(),
            P("fs", "tp"),
            P("tp"),
            P("tp", "fs"),
            P("fs"),
            P(),
            P("fs", "tp"),
            P("tp"),
            P("fs", "tp"),
            P("tp"),
            P("tp", "fs"),
            P("fs"),
        ),
        out_specs=P("fs", "tp"),
        check_vma=False,
    )
```

profile of v0, /device:TPU:0, one launch (start us, length us, event | category | flops | bytes accessed | tf_op | source)
XLA Modules:
  0.0 587.0 jit_solution(10302616835622095069)
XLA Ops:
  6.5 0.0 all-gather.10.cloned.1.call-start
  6.5 0.7 all-gather.10.cloned.1.call-update
  7.3 0.0 all-gather.12.cloned.1.call-start
  7.3 1.6 convert_element_type.145
  8.9 0.0 all-gather.12.cloned.1.call-update
  9.0 0.0 all-gather.14.cloned.1.call-start
  9.0 1.6 convert_element_type.162
  10.6 0.0 all-gather.14.cloned.1.call-update
  10.6 0.0 reduce-scatter.3.cloned.1.call-start
  11.0 22.6 %all-gather = f32[8,1,256]{2,1,0:T(1,128)S(1)} all-gather(f32[1,1,256]{2,1,0:T(1,128)} %bitcast.61), channel_id=1, replica_groups=mesh['fs'=8,'tp'=4] {'fs'}, dimensions={0}, use_global_device_ids=true | all-gather | bytes 9216 | tf_op jit(solution)/shard_map/all_gather | solution.py:84
  33.5 12.6 %all-gather.10.cloned.1.call-done = bf16[1024,2048]{1,0:T(8,128)(2,1)} async-done(((bf16[1024,512]{1,0:T(8,128)(2,1)}), bf16[1024,2048]{1,0:T(8,128)(2,1)}) %all-gather.10.cloned.1.call-update) | async-done | bytes 4194320 | tf_op jit(solution)/shard_map/all_gather | solution.py:43
  46.1 3.1 fusion.1
  49.2 39.4 %all-gather.12.cloned.1.call-done = bf16[2048,256]{1,0:T(8,128)(2,1)} async-done(((bf16[256,256]{1,0:T(8,128)(2,1)}), bf16[2048,256]{1,0:T(8,128)(2,1)}) %all-gather.12.cloned.1.call-update) | async-done | bytes 1048592 | tf_op jit(solution)/shard_map/all_gather | solution.py:88
  88.5 0.0 copy-done.5
  88.5 0.0 copy-done.9
  88.5 3.7 fusion.14
  92.3 1.1 convolution_bitcast_fusion
  93.4 1.1 convolution_bitcast_fusion.1
  94.4 1.1 convolution_bitcast_fusion.2
  95.5 1.1 convolution_bitcast_fusion.3
  96.6 1.5 convolution_select_fusion
  98.1 1.5 convolution_select_fusion.1
  99.6 1.5 convolution_select_fusion.2
  101.1 2.3 fusion.17
  103.4 0.2 copy.22
  103.5 25.2 %all-gather.14.cloned.1.call-done = bf16[256,2048]{1,0:T(8,128)(2,1)} async-done(((bf16[256,256]{1,0:T(8,128)(2,1)}), bf16[256,2048]{1,0:T(8,128)(2,1)}) %all-gather.14.cloned.1.call-update) | async-done | bytes 1048592 | tf_op jit(solution)/shard_map/all_gather | solution.py:58
  128.7 4.5 multiply_convert_fusion.1
  133.3 0.0 reduce-scatter.3.cloned.1.call-update
  133.3 0.0 copy-start.4
  133.3 0.0 all-gather.16.cloned.1.call-start
  133.4 43.5 %reduce-scatter.3.cloned.1.call-done = bf16[1024,512]{1,0:T(8,128)(2,1)} async-done(((bf16[1024,2048]{1,0:T(8,128)(2,1)}), bf16[1024,512]{1,0:T(8,128)(2,1)}) %reduce-scatter.3.cloned.1.call-update) | async-done | bytes 1048592 | tf_op jit(solution)/shard_map/reduce_scatter | solution.py:63
  176.9 0.0 copy-done.1
  176.9 2.5 add_convert_fusion.1
  179.4 0.0 all-gather.16.cloned.1.call-update
  179.4 0.0 copy-start.6
  179.4 0.0 all-gather.18.cloned.1.call-start
  179.5 0.0 copy-done.2
  179.5 1.0 convert_element_type.169
  180.5 0.0 all-gather.18.cloned.1.call-update
  180.5 0.0 all-gather.20.cloned.1.call-start
  180.5 2.4 convert_element_type.170
  182.9 0.0 all-gather.20.cloned.1.call-update
  183.0 0.0 all-gather.22.cloned.1.call-start
  183.0 0.0 copy-done.3
  183.0 1.0 convert_element_type.172
  184.0 0.0 all-gather.22.cloned.1.call-update
  184.0 0.0 reduce-scatter.5.cloned.1.call-start
  184.1 0.0 copy-done.4
  184.1 20.5 %all-gather.1 = f32[8,1,256]{2,1,0:T(1,128)S(1)} all-gather(f32[1,1,256]{2,1,0:T(1,128)S(1)} %bitcast.62), channel_id=1, replica_groups=mesh['fs'=8,'tp'=4] {'fs'}, dimensions={0}, use_global_device_ids=true | all-gather | bytes 9216 | tf_op jit(solution)/shard_map/all_gather | solution.py:85
  204.6 9.4 %all-gather.16.cloned.1.call-done = bf16[1024,2048]{1,0:T(8,128)(2,1)} async-done(((bf16[1024,512]{1,0:T(8,128)(2,1)}), bf16[1024,2048]{1,0:T(8,128)(2,1)}) %all-gather.16.cloned.1.call-update) | async-done | bytes 4194320 | tf_op jit(solution)/shard_map/all_gather | solution.py:43
  214.0 3.1 fusion.3
  217.1 0.0 copy-start.7
  217.1 0.0 copy-start.8
  217.1 97.7 %all-gather.18.cloned.1.call-done = bf16[2048,1536]{1,0:T(8,128)(2,1)} async-done(((bf16[256,1536]{1,0:T(8,128)(2,1)}), bf16[2048,1536]{1,0:T(8,128)(2,1)}) %all-gather.18.cloned.1.call-update) | async-done | bytes 6291472 | tf_op jit(solution)/shard_map/all_gather | solution.py:89
  314.8 0.0 copy-done.6
  314.8 11.7 %fusion.8 = f32[1024,1536]{1,0:T(8,128)} fusion(bf16[2048,1536]{1,0:T(8,128)(2,1)} %all-gather.18.cloned.1.call-done, bf16[1024,2048]{1,0:T(8,128)(2,1)} %all-gather.16.cloned.1.call-done, f32[2048]{0:T(1024)S(1)} %copy-done.6), kind=kOutput, calls=%fused_computation.13 | convolution fusion | flops 6448742400 | bytes 16785408 | tf_op jit(solution)/shard_map/dot_general | solution.py:47
  326.5 87.4 %all-gather.20.cloned.1.call-done = bf16[2048,1536]{1,0:T(8,128)(2,1)} async-done(((bf16[256,1536]{1,0:T(8,128)(2,1)}), bf16[2048,1536]{1,0:T(8,128)(2,1)}) %all-gather.20.cloned.1.call-update) | async-done | bytes 6291472 | tf_op jit(solution)/shard_map/all_gather | solution.py:90
  413.8 99.7 %all-gather.22.cloned.1.call-done = bf16[1536,2048]{1,0:T(8,128)(2,1)} async-done(((bf16[1536,256]{1,0:T(8,128)(2,1)}), bf16[1536,2048]{1,0:T(8,128)(2,1)}) %all-gather.22.cloned.1.call-update) | async-done | bytes 6291472 | tf_op jit(solution)/shard_map/all_gather | solution.py:58
  513.6 0.0 copy-done.7
  513.6 0.0 copy-done.8
  513.6 21.6 %multiply_convert_fusion = bf16[1024,2048]{1,0:T(8,128)(2,1)} fusion(bf16[1536,2048]{1,0:T(8,128)(2,1)} %all-gather.22.cloned.1.call-done, f32[2048]{0:T(1024)S(1)} %bitcast.60, f32[1024,1536]{1,0:T(8,128)} %fusion.8, bf16[2048,1536]{1,0:T(8,128)(2,1)} %all-gather.20.cloned.1.call-done, bf16[1024,2048]{1,0:T(8,128)(2,1)} %all-gather.16.cloned.1.call-done, ...), kind=kOutput, calls=%fused_computation.8 | convolution fusion | flops 12911116288 | bytes 27295744 | tf_op jit(solution)/shard_map/dot_general | solution.py:56
  535.2 0.0 reduce-scatter.5.cloned.1.call-update
  535.2 42.8 %reduce-scatter.5.cloned.1.call-done = bf16[1024,512]{1,0:T(8,128)(2,1)} async-done(((bf16[1024,2048]{1,0:T(8,128)(2,1)}), bf16[1024,512]{1,0:T(8,128)(2,1)}) %reduce-scatter.5.cloned.1.call-update) | async-done | bytes 1048592 | tf_op jit(solution)/shard_map/reduce_scatter | solution.py:63
  578.0 2.5 add_convert_fusion
  (27 shorter events, 0.2 us)
Async XLA Ops:
  6.5 82.0 %copy-start.5 = (f32[2048]{0:T(1024)S(1)}, f32[2048]{0:T(1024)}, u32[]{:S(2)}) copy-start(f32[2048]{0:T(1024)} %param.14) | copy-start | bytes 24580
  6.5 82.0 %copy-start.9 = (f32[256]{0:T(256)S(1)}, f32[256]{0:T(256)}, u32[]{:S(2)}) copy-start(f32[256]{0:T(256)} %param.16) | copy-start | bytes 3076
  6.5 39.6 %all-gather.10.cloned.1.call-start = ((), (), s32[]{:S(2)}) async-start(), calls=%async_computation.2 | async-start | bytes 5242880 | tf_op jit(solution)/shard_map/all_gather | solution.py:43
  7.3 81.3 %all-gather.12.cloned.1.call-start = ((), (), s32[]{:S(2)}) async-start(), calls=%async_computation.3 | async-start | bytes 1179648 | tf_op jit(solution)/shard_map/all_gather | solution.py:88
  9.0 119.8 %all-gather.14.cloned.1.call-start = ((), (), s32[]{:S(2)}) async-start(), calls=%async_computation.4 | async-start | bytes 1179648 | tf_op jit(solution)/shard_map/all_gather | solution.py:58
  10.6 166.2 %reduce-scatter.3.cloned.1.call-start = ((), (), s32[]{:S(2)}) async-start(), calls=%async_computation.5 | async-start | bytes 5242880 | tf_op jit(solution)/shard_map/reduce_scatter | solution.py:63
  128.7 48.1 %copy-start.1 = (bf16[1024,512]{1,0:T(8,128)(2,1)S(1)}, bf16[1024,512]{1,0:T(8,128)(2,1)}, u32[]{:S(2)}) copy-start(bf16[1024,512]{1,0:T(8,128)(2,1)} %param.13) | copy-start | bytes 3145732
  133.3 46.2 %copy-start.2 = (f32[256,1536]{1,0:T(8,128)S(1)}, f32[256,1536]{1,0:T(8,128)}, u32[]{:S(2)}) copy-start(f32[256,1536]{1,0:T(8,128)} %param.20) | copy-start | bytes 4718596
  133.3 50.8 %copy-start.4 = (f32[256]{0:T(256)S(1)}, f32[256]{0:T(256)}, u32[]{:S(2)}) copy-start(f32[256]{0:T(256)} %param.25) | copy-start | bytes 3076
  133.3 80.7 %all-gather.16.cloned.1.call-start = ((), (), s32[]{:S(2)}) async-start(), calls=%async_computation.6 | async-start | bytes 5242880 | tf_op jit(solution)/shard_map/all_gather | solution.py:43
  179.4 3.6 copy-start.3
  179.4 135.4 %copy-start.6 = (f32[2048]{0:T(1024)S(1)}, f32[2048]{0:T(1024)}, u32[]{:S(2)}) copy-start(f32[2048]{0:T(1024)} %param.19) | copy-start | bytes 24580
  179.4 135.4 %all-gather.18.cloned.1.call-start = ((), (), s32[]{:S(2)}) async-start(), calls=%async_computation.7 | async-start | bytes 7077888 | tf_op jit(solution)/shard_map/all_gather | solution.py:89
  180.5 233.4 %all-gather.20.cloned.1.call-start = ((), (), s32[]{:S(2)}) async-start(), calls=%async_computation.8 | async-start | bytes 7077888 | tf_op jit(solution)/shard_map/all_gather | solution.py:90
  183.0 330.6 %all-gather.22.cloned.1.call-start = ((), (), s32[]{:S(2)}) async-start(), calls=%async_computation.9 | async-start | bytes 7077888 | tf_op jit(solution)/shard_map/all_gather | solution.py:58
  184.0 394.0 %reduce-scatter.5.cloned.1.call-start = ((), (), s32[]{:S(2)}) async-start(), calls=%async_computation.10 | async-start | bytes 5242880 | tf_op jit(solution)/shard_map/reduce_scatter | solution.py:63
  217.1 296.5 %copy-start.7 = (f32[1536]{0:T(1024)S(1)}, f32[1536]{0:T(1024)}, u32[]{:S(2)}) copy-start(f32[1536]{0:T(1024)} %param.23) | copy-start | bytes 18436
  217.1 296.5 %copy-start.8 = (f32[1536]{0:T(1024)S(1)}, f32[1536]{0:T(1024)}, u32[]{:S(2)}) copy-start(f32[1536]{0:T(1024)} %param.21) | copy-start | bytes 18436
  513.6 64.4 %copy-start = (bf16[1024,512]{1,0:T(8,128)(2,1)S(1)}, bf16[1024,512]{1,0:T(8,128)(2,1)}, u32[]{:S(2)}) copy-start(bf16[1024,512]{1,0:T(8,128)(2,1)} %add_convert_fusion.1) | copy-start | bytes 3145732
Sparse Core Ops, SparseCore 0:
  8.9 37.1 all-gather.9
  48.2 40.2 all-gather.11
  90.6 38.0 all-gather.13
  133.4 43.4 reduce-scatter.2
  179.5 34.4 all-gather.15
  216.0 98.6 all-gather.17
  316.9 96.8 all-gather.19
  415.9 97.6 all-gather.21
  535.3 42.5 reduce-scatter.4
where the time goes:
time: 587 us
  waiting for transfers between devices  458 us (78%)
  matrix products  52.6 us (9%)
  blocking collectives  43.1 us (7%)
  other arithmetic  18.9 us (3%)
  between operations  13.5 us (2%)
    all_gather x2, waiting for transfers between devices, column_product(): lax.all_gather(weight_columns, 'fs', axis=1, tiled=True)  125 us
    all_gather x1, waiting for transfers between devices, local(): lax.all_gather(gate_weight.astype(jnp.bfloat16), 'fs', axis=0, tiled=True)  97.7 us
    all_gather x1, waiting for transfers between devices, local(): lax.all_gather(up_weight.astype(jnp.bfloat16), 'fs', axis=0, tiled=True)  87.4 us
    reduce_scatter x2, waiting for transfers between devices, column_product(): lax.psum_scatter(partial_value.astype(jnp.bfloat16), 'tp', scatter_dimens...  86.3 us
    all_gather x1, waiting for transfers between devices, local(): lax.all_gather(in_weight.astype(jnp.bfloat16), 'fs', axis=0, tiled=True)  39.4 us
    dot_general x2, matrix products, column_product(): jnp.dot(hidden, lax.all_gather(weight_columns, 'fs', axis=1, tiled=True),...  26.1 us
    all_gather x1, blocking collectives, local(): lax.all_gather(out_scale, 'fs', axis=0, tiled=True)  22.6 us
    all_gather x2, waiting for transfers between devices, fold_rows(): lax.all_gather(features, 'tp', axis=1, tiled=True).astype(jnp.float32)  22 us
  transfers between devices with their start and end apart: 9, of which 9 were waited for; matrix products, arithmetic and copies ran while one was open for 7% of the time, Pallas kernels for 0%

commit v1 on v0

--- a/solution.py
+++ b/solution.py
@@ -9,6 +9,18 @@
 GC = 256
 WINDOWS = (2, 4, 8, 16)
 EPSILON = 1e-06
+
+
+def gather_by_bits(value, axis, dim):
+    ways, here = (lax.axis_size(axis), lax.axis_index(axis))
+    grown, reach = (value, 1)
+    while reach < ways:
+        theirs = lax.ppermute(grown, axis, [(d, d ^ reach) for d in range(ways)])
+        mine_first = jnp.concatenate([grown, theirs], axis=dim)
+        theirs_first = jnp.concatenate([theirs, grown], axis=dim)
+        grown = jnp.where(here & reach == 0, mine_first, theirs_first)
+        reach = 2 * reach
+    return grown
 
 
 def box_matrix(length, window):
@@ -85,7 +97,7 @@
         lax.all_gather(down_scale, "fs", axis=0, tiled=True),
     )
     in_full, gate_full, up_full = (
-        lax.all_gather(in_weight.astype(jnp.bfloat16), "fs", axis=0, tiled=True),
+        gather_by_bits(in_weight.astype(jnp.bfloat16), "fs", 0),
         lax.all_gather(gate_weight.astype(jnp.bfloat16), "fs", axis=0, tiled=True),
         lax.all_gather(up_weight.astype(jnp.bfloat16), "fs", axis=0, tiled=True),
     )

time: 587 us -> 546 us (0.930)
  waiting for transfers between devices: 458 us -> 415 us
    all_gather x1 -> x0, waiting for transfers between devices: 39.4 us -> none  [local(): lax.all_gather(in_weight.astype(jnp.bfloat16), 'fs', axis=0, tiled=True)]
    ppermute x0 -> x3, waiting for transfers between devices: none -> 9.03 us  [gather_by_bits(): theirs = lax.ppermute(grown, axis, [(d, d ^ reach) for d in range(ways)])]
    all_gather x2, waiting for transfers between devices: 125 us -> 116 us  [column_product(): lax.all_gather(weight_columns, 'fs', axis=1, tiled=True)]
  transfers between devices with their start and end apart: 9 -> 11, of which waited for: 9 -> 10; matrix products, arithmetic and copies ran while one was open for 7% -> 7% of each run, Pallas kernels for 0% -> 0%
where the time goes in v1:
time: 546 us
  waiting for transfers between devices  415 us (76%)
  matrix products  52.3 us (10%)
  blocking collectives  40.5 us (7%)
  other arithmetic  18.6 us (3%)
  between operations  13.8 us (3%)
    all_gather x2, waiting for transfers between devices, column_product(): lax.all_gather(weight_columns, 'fs', axis=1, tiled=True)  116 us
    all_gather x1, waiting for transfers between devices, local(): lax.all_gather(gate_weight.astype(jnp.bfloat16), 'fs', axis=0, tiled=True)  97.7 us
    all_gather x1, waiting for transfers between devices, local(): lax.all_gather(up_weight.astype(jnp.bfloat16), 'fs', axis=0, tiled=True)  87.2 us
    reduce_scatter x2, waiting for transfers between devices, column_product(): lax.psum_scatter(partial_value.astype(jnp.bfloat16), 'tp', scatter_dimens...  86.3 us
    dot_general x2, matrix products, column_product(): jnp.dot(hidden, lax.all_gather(weight_columns, 'fs', axis=1, tiled=True),...  26.1 us
    all_gather x1, blocking collectives, local(): lax.all_gather(down_scale, 'fs', axis=0, tiled=True)  20.5 us
    all_gather x1, blocking collectives, local(): lax.all_gather(out_scale, 'fs', axis=0, tiled=True)  20.1 us
    all_gather x2, waiting for transfers between devices, fold_rows(): lax.all_gather(features, 'tp', axis=1, tiled=True).astype(jnp.float32)  18.3 us
  transfers between devices with their start and end apart: 11, of which 10 were waited for; matrix products, arithmetic and copies ran while one was open for 7% of the time, Pallas kernels for 0%

profile of v1, /device:TPU:0, one launch (start us, length us, event | category | flops | bytes accessed | tf_op | source)
XLA Modules:
  0.0 546.0 jit_solution(5732679175274013854)
XLA Ops:
  6.5 0.0 all-gather.9.cloned.1.call-start
  6.5 0.7 all-gather.9.cloned.1.call-update
  7.3 0.0 all-gather.11.cloned.1.call-start
  7.3 1.0 convert_element_type.145
  8.3 3.1 collective-permute-start
  11.3 1.6 convert_element_type.162
  13.0 0.0 all-gather.11.cloned.1.call-update
  13.0 0.0 reduce-scatter.3.cloned.1.call-start
  13.3 1.6 collective-permute-done
  14.8 0.1 maximum_select_fusion.3
  14.9 1.9 collective-permute-start.1
  16.8 20.1 %all-gather = f32[8,1,256]{2,1,0:T(1,128)S(1)} all-gather(f32[1,1,256]{2,1,0:T(1,128)} %bitcast.60), channel_id=1, replica_groups=mesh['fs'=8,'tp'=4] {'fs'}, dimensions={0}, use_global_device_ids=true | all-gather | bytes 9216 | tf_op jit(solution)/shard_map/all_gather | solution.py:96
  36.9 0.0 collective-permute-done.1
  36.9 0.2 maximum_select_fusion.2
  37.1 0.1 collective-permute-start.2
  37.2 8.9 %all-gather.9.cloned.1.call-done = bf16[1024,2048]{1,0:T(8,128)(2,1)} async-done(((bf16[1024,512]{1,0:T(8,128)(2,1)}), bf16[1024,2048]{1,0:T(8,128)(2,1)}) %all-gather.9.cloned.1.call-update) | async-done | bytes 4194320 | tf_op jit(solution)/shard_map/all_gather | solution.py:55
  46.1 3.1 fusion.1
  49.2 7.5 %collective-permute-done.2 = bf16[1024,256]{1,0:T(8,128)(2,1)S(1)} collective-permute-done((bf16[1024,256]{1,0:T(8,128)(2,1)S(1)}, bf16[1024,256]{1,0:T(8,128)(2,1)S(1)}, u32[]{:S(2)}, u32[]{:S(2)}) %collective-permute-start.2) | collective-permute-done | bytes 524320 | tf_op jit(solution)/shard_map/ppermute | solution.py:18
  56.7 0.0 copy-done.5
  56.7 0.0 copy-done.9
  56.7 3.5 fusion.14
  60.1 1.1 convolution_bitcast_fusion
  61.2 1.0 convolution_bitcast_fusion.1
  62.3 1.1 convolution_bitcast_fusion.2
  63.3 1.1 convolution_bitcast_fusion.3
  64.4 1.5 convolution_select_fusion
  65.9 1.5 convolution_select_fusion.1
  67.4 1.5 convolution_select_fusion.2
  68.9 2.3 fusion.17
  71.2 0.2 copy.22
  71.3 16.2 %all-gather.11.cloned.1.call-done = bf16[256,2048]{1,0:T(8,128)(2,1)} async-done(((bf16[256,256]{1,0:T(8,128)(2,1)}), bf16[256,2048]{1,0:T(8,128)(2,1)}) %all-gather.11.cloned.1.call-update) | async-done | bytes 1048592 | tf_op jit(solution)/shard_map/all_gather | solution.py:70
  87.6 4.5 multiply_convert_fusion.1
  92.1 0.0 reduce-scatter.3.cloned.1.call-update
  92.1 0.0 copy-start.4
  92.2 0.0 all-gather.13.cloned.1.call-start
  92.2 43.5 %reduce-scatter.3.cloned.1.call-done = bf16[1024,512]{1,0:T(8,128)(2,1)} async-done(((bf16[1024,2048]{1,0:T(8,128)(2,1)}), bf16[1024,512]{1,0:T(8,128)(2,1)}) %reduce-scatter.3.cloned.1.call-update) | async-done | bytes 1048592 | tf_op jit(solution)/shard_map/reduce_scatter | solution.py:75
  135.7 0.0 copy-done.1
  135.7 2.5 add_convert_fusion.1
  138.2 0.0 all-gather.13.cloned.1.call-update
  138.2 0.0 copy-start.6
  138.2 0.0 all-gather.15.cloned.1.call-start
  138.3 1.0 convert_element_type.169
  139.3 0.0 all-gather.15.cloned.1.call-update
  139.3 0.0 all-gather.17.cloned.1.call-start
  139.4 2.4 convert_element_type.170
  141.8 0.0 all-gather.17.cloned.1.call-update
  141.8 0.0 all-gather.19.cloned.1.call-start
  141.9 1.0 convert_element_type.172
  142.8 0.0 all-gather.19.cloned.1.call-update
  142.9 0.0 reduce-scatter.5.cloned.1.call-start
  142.9 20.5 %all-gather.1 = f32[8,1,256]{2,1,0:T(1,128)S(1)} all-gather(f32[1,1,256]{2,1,0:T(1,128)S(1)} %bitcast.61), channel_id=1, replica_groups=mesh['fs'=8,'tp'=4] {'fs'}, dimensions={0}, use_global_device_ids=true | all-gather | bytes 9216 | tf_op jit(solution)/shard_map/all_gather | solution.py:97
  163.4 9.4 %all-gather.13.cloned.1.call-done = bf16[1024,2048]{1,0:T(8,128)(2,1)} async-done(((bf16[1024,512]{1,0:T(8,128)(2,1)}), bf16[1024,2048]{1,0:T(8,128)(2,1)}) %all-gather.13.cloned.1.call-update) | async-done | bytes 4194320 | tf_op jit(solution)/shard_map/all_gather | solution.py:55
  172.8 3.1 fusion.3
  175.9 0.0 copy-start.7
  175.9 0.0 copy-start.8
  175.9 97.7 %all-gather.15.cloned.1.call-done = bf16[2048,1536]{1,0:T(8,128)(2,1)} async-done(((bf16[256,1536]{1,0:T(8,128)(2,1)}), bf16[2048,1536]{1,0:T(8,128)(2,1)}) %all-gather.15.cloned.1.call-update) | async-done | bytes 6291472 | tf_op jit(solution)/shard_map/all_gather | solution.py:101
  273.6 11.7 %fusion.8 = f32[1024,1536]{1,0:T(8,128)} fusion(bf16[2048,1536]{1,0:T(8,128)(2,1)} %all-gather.15.cloned.1.call-done, bf16[1024,2048]{1,0:T(8,128)(2,1)} %all-gather.13.cloned.1.call-done, f32[2048]{0:T(1024)S(1)} %copy-done.6), kind=kOutput, calls=%fused_computation.13 | convolution fusion | flops 6448742400 | bytes 16785408 | tf_op jit(solution)/shard_map/dot_general | solution.py:59
  285.3 87.2 %all-gather.17.cloned.1.call-done = bf16[2048,1536]{1,0:T(8,128)(2,1)} async-done(((bf16[256,1536]{1,0:T(8,128)(2,1)}), bf16[2048,1536]{1,0:T(8,128)(2,1)}) %all-gather.17.cloned.1.call-update) | async-done | bytes 6291472 | tf_op jit(solution)/shard_map/all_gather | solution.py:102
  372.5 99.7 %all-gather.19.cloned.1.call-done = bf16[1536,2048]{1,0:T(8,128)(2,1)} async-done(((bf16[1536,256]{1,0:T(8,128)(2,1)}), bf16[1536,2048]{1,0:T(8,128)(2,1)}) %all-gather.19.cloned.1.call-update) | async-done | bytes 6291472 | tf_op jit(solution)/shard_map/all_gather | solution.py:70
  472.3 21.6 %multiply_convert_fusion = bf16[1024,2048]{1,0:T(8,128)(2,1)} fusion(bf16[1536,2048]{1,0:T(8,128)(2,1)} %all-gather.19.cloned.1.call-done, f32[2048]{0:T(1024)S(1)} %bitcast.59, f32[1024,1536]{1,0:T(8,128)} %fusion.8, bf16[2048,1536]{1,0:T(8,128)(2,1)} %all-gather.17.cloned.1.call-done, bf16[1024,2048]{1,0:T(8,128)(2,1)} %all-gather.13.cloned.1.call-done, ...), kind=kOutput, calls=%fused_computation.8 | convolution fusion | flops 12911116288 | bytes 27295744 | tf_op jit(solution)/shard_map/dot_general | solution.py:68
  493.9 0.0 reduce-scatter.5.cloned.1.call-update
  493.9 42.8 %reduce-scatter.5.cloned.1.call-done = bf16[1024,512]{1,0:T(8,128)(2,1)} async-done(((bf16[1024,2048]{1,0:T(8,128)(2,1)}), bf16[1024,512]{1,0:T(8,128)(2,1)}) %reduce-scatter.5.cloned.1.call-update) | async-done | bytes 1048592 | tf_op jit(solution)/shard_map/reduce_scatter | solution.py:75
  536.7 0.0 copy-done
  536.7 2.5 add_convert_fusion
  (33 shorter events, 0.2 us)
Async XLA Ops:
  6.5 50.1 %copy-start.5 = (f32[2048]{0:T(1024)S(1)}, f32[2048]{0:T(1024)}, u32[]{:S(2)}) copy-start(f32[2048]{0:T(1024)} %param.14) | copy-start | bytes 24580
  6.5 50.1 %copy-start.9 = (f32[256]{0:T(256)S(1)}, f32[256]{0:T(256)}, u32[]{:S(2)}) copy-start(f32[256]{0:T(256)} %param.16) | copy-start | bytes 3076
  6.5 39.6 %all-gather.9.cloned.1.call-start = ((), (), s32[]{:S(2)}) async-start(), calls=%async_computation.2 | async-start | bytes 5242880 | tf_op jit(solution)/shard_map/all_gather | solution.py:55
  7.3 80.3 %all-gather.11.cloned.1.call-start = ((), (), s32[]{:S(2)}) async-start(), calls=%async_computation.3 | async-start | bytes 1179648 | tf_op jit(solution)/shard_map/all_gather | solution.py:70
  8.3 6.6 %collective-permute-start = (bf16[256,256]{1,0:T(8,128)(2,1)S(1)}, bf16[256,256]{1,0:T(8,128)(2,1)S(1)}, u32[]{:S(2)}, u32[]{:S(2)}) collective-permute-start(bf16[256,256]{1,0:T(8,128)(2,1)S(1)} %convert_element_type.145), channel_id=1, source_target_pairs={{0,4},{4,0},{8,12},{12,8},{16,20},{20,16},{24,28},{28,24},{1,5},{5... | collective-permute-start | bytes 393224 | tf_op jit(solution)/shard_map/ppermute | solution.py:18
  13.0 122.7 %reduce-scatter.3.cloned.1.call-start = ((), (), s32[]{:S(2)}) async-start(), calls=%async_computation.4 | async-start | bytes 5242880 | tf_op jit(solution)/shard_map/reduce_scatter | solution.py:75
  14.9 21.9 %collective-permute-start.1 = (bf16[512,256]{1,0:T(8,128)(2,1)S(1)}, bf16[512,256]{1,0:T(8,128)(2,1)S(1)}, u32[]{:S(2)}, u32[]{:S(2)}) collective-permute-start(bf16[512,256]{1,0:T(8,128)(2,1)S(1)} %maximum_select_fusion.3), channel_id=1, source_target_pairs={{0,8},{4,12},{8,0},{12,4},{16,24},{20,28},{24,16},{28,20},{1,9},{5... | collective-permute-start | bytes 786440 | tf_op jit(solution)/shard_map/ppermute | solution.py:18
  37.1 19.5 %collective-permute-start.2 = (bf16[1024,256]{1,0:T(8,128)(2,1)S(1)}, bf16[1024,256]{1,0:T(8,128)(2,1)S(1)}, u32[]{:S(2)}, u32[]{:S(2)}) collective-permute-start(bf16[1024,256]{1,0:T(8,128)(2,1)S(1)} %maximum_select_fusion.2), channel_id=1, source_target_pairs={{0,16},{4,20},{8,24},{12,28},{16,0},{20,4},{24,8},{28,12},{1,17},{... | collective-permute-start | bytes 1572872 | tf_op jit(solution)/shard_map/ppermute | solution.py:18
  87.6 48.1 %copy-start.1 = (bf16[1024,512]{1,0:T(8,128)(2,1)S(1)}, bf16[1024,512]{1,0:T(8,128)(2,1)}, u32[]{:S(2)}) copy-start(bf16[1024,512]{1,0:T(8,128)(2,1)} %param.13) | copy-start | bytes 3145732
  92.1 46.2 %copy-start.2 = (f32[256,1536]{1,0:T(8,128)S(1)}, f32[256,1536]{1,0:T(8,128)}, u32[]{:S(2)}) copy-start(f32[256,1536]{1,0:T(8,128)} %param.20) | copy-start | bytes 4718596
  92.1 50.8 %copy-start.4 = (f32[256]{0:T(256)S(1)}, f32[256]{0:T(256)}, u32[]{:S(2)}) copy-start(f32[256]{0:T(256)} %param.25) | copy-start | bytes 3076
  92.2 80.7 %all-gather.13.cloned.1.call-start = ((), (), s32[]{:S(2)}) async-start(), calls=%async_computation.5 | async-start | bytes 5242880 | tf_op jit(solution)/shard_map/all_gather | solution.py:55
  138.2 3.7 copy-start.3
  138.2 135.4 %copy-start.6 = (f32[2048]{0:T(1024)S(1)}, f32[2048]{0:T(1024)}, u32[]{:S(2)}) copy-start(f32[2048]{0:T(1024)} %param.19) | copy-start | bytes 24580
  138.2 135.4 %all-gather.15.cloned.1.call-start = ((), (), s32[]{:S(2)}) async-start(), calls=%async_computation.6 | async-start | bytes 7077888 | tf_op jit(solution)/shard_map/all_gather | solution.py:101
  139.3 233.2 %all-gather.17.cloned.1.call-start = ((), (), s32[]{:S(2)}) async-start(), calls=%async_computation.7 | async-start | bytes 7077888 | tf_op jit(solution)/shard_map/all_gather | solution.py:102
  141.8 330.5 %all-gather.19.cloned.1.call-start = ((), (), s32[]{:S(2)}) async-start(), calls=%async_computation.8 | async-start | bytes 7077888 | tf_op jit(solution)/shard_map/all_gather | solution.py:70
  142.9 393.8 %reduce-scatter.5.cloned.1.call-start = ((), (), s32[]{:S(2)}) async-start(), calls=%async_computation.9 | async-start | bytes 5242880 | tf_op jit(solution)/shard_map/reduce_scatter | solution.py:75
  175.9 296.4 %copy-start.7 = (f32[1536]{0:T(1024)S(1)}, f32[1536]{0:T(1024)}, u32[]{:S(2)}) copy-start(f32[1536]{0:T(1024)} %param.23) | copy-start | bytes 18436
  175.9 296.3 %copy-start.8 = (f32[1536]{0:T(1024)S(1)}, f32[1536]{0:T(1024)}, u32[]{:S(2)}) copy-start(f32[1536]{0:T(1024)} %param.21) | copy-start | bytes 18436
  472.3 64.4 %copy-start = (bf16[1024,512]{1,0:T(8,128)(2,1)S(1)}, bf16[1024,512]{1,0:T(8,128)(2,1)}, u32[]{:S(2)}) copy-start(bf16[1024,512]{1,0:T(8,128)(2,1)} %add_convert_fusion.1) | copy-start | bytes 3145732
Sparse Core Ops, SparseCore 0:
  8.9 37.1 all-gather.8
  48.1 39.3 all-gather.10
  92.3 43.4 reduce-scatter.2
  138.3 34.4 all-gather.12
  174.9 98.6 all-gather.14
  275.6 96.8 all-gather.16
  374.6 97.6 all-gather.18
  494.0 42.5 reduce-scatter.4
